TPU v7x, 32 devices: a whole 2x2x4 slice. The times are simulated.
32 devices in a mesh: ep: 8 (over z, x), tp: 4 (over y, core).
Axes of the slice: x: 2, y: 2, z: 4, core: 2. Of those that a mesh axis runs over, the one named last changes fastest.
Arguments:
- tokens: bfloat16 [1024, 2048], P('ep', 'tp'), may hold values from -36 to 36
- cotangent: bfloat16 [1024, 2048], P('ep', 'tp'), may hold values from -6 to 6
- routes: int32 [1024, 2], P('ep'), may hold values from 0 to 7, all different within a row; in each aligned block of 128 rows (0 to 127, 128 to 255, ...) at most 33 rows name the same one
- route_weights: bfloat16 [1024, 2], P('ep'), may hold values from 0.099609375 to 1
- gate_weight: bfloat16 [8, 2048, 1024], P('ep', None, 'tp'), may hold values from -0.125 to 0.125
- up_weight: bfloat16 [8, 2048, 1024], P('ep', None, 'tp'), may hold values from -0.125 to 0.125
- down_weight: bfloat16 [8, 1024, 2048], P('ep', 'tp'), may hold values from -0.1875 to 0.1875
Outputs:
- token_grad: bfloat16 [1024, 2048], P('ep', 'tp')
- weight_grad: bfloat16 [1024, 2], P('ep')
- down_grad: bfloat16 [8, 1024, 2048], P('ep', 'tp')
Inputs may be any that keep to these rules, and one draw needn't show every extreme that they name: `routes`: each row names 2 different experts; within the rows of one device of ep (aligned blocks of 128 rows) no expert is named more than 33 times.
All inputs are finite; a program needn't handle non-finite values.
Results may differ from a plain program's by a relative error of at most 0.013.
Values may be sent and summed in bfloat16 or wider, within the bound.
A program may use at most 64 MiB of HBM per device.

v0:
```python
import jax
import jax.numpy as jnp
from jax import lax
from jax.sharding import PartitionSpec as P

clamp_limit = 7.0
alpha_gate = 1.702


def ranks_within(route_block, experts):
    flat_routes = route_block.reshape(-1)
    onehot = (flat_routes[:, None] == jnp.arange(experts, dtype=jnp.int32)[None, :]).astype(
        jnp.int32
    )
    before = jnp.cumsum(onehot, axis=0) - onehot
    return jnp.sum(before * onehot, axis=1)


def expert_terms(exp_rows, exp_grads, scales, gate_mat, up_mat, down_mat):
    gate_pre = jnp.dot(exp_rows, gate_mat, preferred_element_type=jnp.float32)
    up_pre = jnp.dot(exp_rows, up_mat, preferred_element_type=jnp.float32)
    gate_clip = jnp.minimum(gate_pre, clamp_limit)
    up_clip = jnp.clip(up_pre, -clamp_limit, clamp_limit)
    sigmoid_gate = jax.nn.sigmoid(alpha_gate * gate_clip)
    swish_gate = gate_clip * sigmoid_gate
    hidden = (up_clip + 1.0) * swish_gate
    back_proj = lax.dot_general(
        exp_grads, down_mat, (((1,), (1,)), ((), ())), preferred_element_type=jnp.float32
    )
    scores = jnp.sum(hidden * back_proj, axis=1)
    weight_col = scales.astype(jnp.float32)[:, None]
    scaled = back_proj * weight_col
    slope = sigmoid_gate + alpha_gate * swish_gate * (1.0 - sigmoid_gate)
    gate_grad = jnp.where(gate_pre < clamp_limit, scaled * (up_clip + 1.0) * slope, 0.0).astype(
        jnp.bfloat16
    )
    up_grad = jnp.where(jnp.abs(up_pre) < clamp_limit, scaled * swish_gate, 0.0).astype(
        jnp.bfloat16
    )
    weighted = (hidden * weight_col).astype(jnp.bfloat16)
    down_part = lax.dot_general(
        weighted, exp_grads, (((0,), (0,)), ((), ())), preferred_element_type=jnp.float32
    )
    token_part = lax.dot_general(
        gate_grad, gate_mat, (((1,), (1,)), ((), ())), preferred_element_type=jnp.float32
    )
    token_part = token_part + lax.dot_general(
        up_grad, up_mat, (((1,), (1,)), ((), ())), preferred_element_type=jnp.float32
    )
    return (token_part, scores, down_part)


def per_device(tokens, cotangent, routes, route_weights, gate_weight, up_weight, down_weight):
    experts = lax.axis_size("ep")
    tok_rows, top_count = routes.shape
    slots_each = tok_rows * top_count // experts + 1
    slot_count = experts * slots_each
    slot_ranks = ranks_within(routes, experts)
    slot_place = routes.reshape(-1) * slots_each + slot_ranks
    slot_owner = jnp.full((slot_count,), -1, jnp.int32)
    slot_owner = slot_owner.at[slot_place].set(jnp.arange(tok_rows * top_count, dtype=jnp.int32))
    filled = slot_owner >= 0
    pair_index = jnp.where(filled, slot_owner, 0)
    token_index = pair_index // top_count
    send_scales = jnp.where(filled, route_weights.reshape(-1)[pair_index], 0)
    send_rows = jnp.where(filled[:, None], tokens[token_index], 0)
    send_grads = jnp.where(filled[:, None], cotangent[token_index], 0)
    part_rows, part_grads, scales = (
        lax.all_to_all(send_rows, "ep", split_axis=0, concat_axis=0, tiled=True),
        lax.all_to_all(send_grads, "ep", split_axis=0, concat_axis=0, tiled=True),
        lax.all_to_all(send_scales, "ep", split_axis=0, concat_axis=0, tiled=True),
    )
    exp_rows, exp_grads = (
        lax.all_gather(part_rows, "tp", axis=1, tiled=True),
        lax.all_gather(part_grads, "tp", axis=1, tiled=True),
    )
    token_part, scores, down_part = expert_terms(
        exp_rows, exp_grads, scales, gate_weight[0], up_weight[0], down_weight[0]
    )
    token_share = lax.psum_scatter(
        token_part.astype(jnp.bfloat16), "tp", scatter_dimension=1, tiled=True
    )
    score_total = lax.psum(scores, "tp")
    back_rows, back_scores = (
        lax.all_to_all(token_share, "ep", split_axis=0, concat_axis=0, tiled=True),
        lax.all_to_all(
            score_total.astype(jnp.bfloat16), "ep", split_axis=0, concat_axis=0, tiled=True
        ),
    )
    pair_rows = back_rows[slot_place].reshape(tok_rows, top_count, back_rows.shape[1])
    token_grad = jnp.sum(pair_rows.astype(jnp.float32), axis=1).astype(jnp.bfloat16)
    weight_grad = back_scores[slot_place].reshape(tok_rows, top_count)
    return (token_grad, weight_grad, down_part.astype(jnp.bfloat16)[None])


def solution(mesh):
    placed = (
        P("ep", "tp"),
        P("ep", "tp"),
        P("ep", None),
        P("ep", None),
        P("ep", None, "tp"),
        P("ep", None, "tp"),
        P("ep", "tp", None),
    )
    return jax.shard_map(
        per_device,
        mesh=mesh,
        in_specs=placed,
        out_specs=(P("ep", "tp"), P("ep", None), P("ep", "tp", None)),
        check_vma=False,
    )
```

profile of v0, /device:TPU:0, one launch (start us, length us, event | category | flops | bytes accessed | tf_op | source)
XLA Modules:
  0.0 125.2 jit_solution(2446107210826918145)
XLA Ops:
  7.2 0.9 copy.16
  8.1 0.1 eq.29
  8.3 0.1 eq.25
  8.4 0.7 broadcast_multiply_fusion
  9.1 0.6 reduce-window.6
  9.7 0.2 slice_reduce_fusion
  9.9 0.1 copy.15
  10.0 0.1 mul.62
  10.2 0.1 fusion.24
  10.3 1.4 %scatter_custom_fusion = s32[264]{0:T(512)S(1)} fusion(s32[256]{0:T(256)S(1)} %bitcast.31, s32[256]{0:T(256)S(1)} %iota.11, s32[]{:T(128)} %constant.13.clone.1), kind=kCustom, calls=%fused_computation.62 | custom fusion | bytes 1060 | tf_op jit(solution)/shard_map/scatter | solution.py:61
  11.7 0.1 broadcast_in_dim.50
  11.8 2.0 %gather_fusion = bf16[264,512]{1,0:T(8,128)(2,1)S(1)} fusion(bf16[128,512]{1,0:T(8,128)(2,1)S(1)} %copy-done.1, s32[1024]{0:T(1024)S(1)} %pad_clamp_fusion.2), kind=kCustom, calls=%fused_computation | custom fusion | bytes 541728 | tf_op jit(solution)/shard_map/gather | solution.py:66
  13.8 0.1 gather.20
  13.9 2.0 %gather_fusion.1 = bf16[264,512]{1,0:T(8,128)(2,1)S(1)} fusion(bf16[128,512]{1,0:T(8,128)(2,1)S(1)} %copy-done.2, s32[1024]{0:T(1024)S(1)} %pad_clamp_fusion.2), kind=kCustom, calls=%fused_computation.1 | custom fusion | bytes 541728 | tf_op jit(solution)/shard_map/gather | solution.py:67
  15.9 0.1 gather.22
  16.0 0.1 broadcast_select_fusion
  16.2 18.0 %all_to_all.53 = bf16[8,33,512]{2,1,0:T(8,128)(2,1)S(1)} all-to-all(bf16[8,33,512]{2,1,0:T(8,128)(2,1)S(1)} %get-tuple-element.12), channel_id=1, replica_groups=mesh['ep'=8,'tp'=4] {'ep'}, dimensions={0} | all-to-all | bytes 540672 | tf_op jit(solution)/shard_map/all_to_all | solution.py:69
  34.2 0.8 all_to_all.35
  35.0 13.6 %all_to_all.54 = bf16[8,33,512]{2,1,0:T(8,128)(2,1)S(1)} all-to-all(bf16[8,33,512]{2,1,0:T(8,128)(2,1)S(1)} %get-tuple-element.11), channel_id=1, replica_groups=mesh['ep'=8,'tp'=4] {'ep'}, dimensions={0} | all-to-all | bytes 540672 | tf_op jit(solution)/shard_map/all_to_all | solution.py:70
  48.7 0.8 all_to_all.37
  49.6 0.1 copy.18
  49.7 0.1 reshape.91
  49.9 2.4 %gather_fusion.2 = bf16[264]{0:T(512)(128)(2,1)S(1)} fusion(bf16[256]{0:T(256)(128)(2,1)S(1)} %reshape.91, s32[1024]{0:T(1024)S(1)} %pad_clamp_fusion.1), kind=kCustom, calls=%fused_computation.2 | custom fusion | bytes 2112 | tf_op jit(solution)/shard_map/gather | solution.py:65
  52.3 0.1 all_to_all.46
  52.4 9.2 %all_to_all.55 = bf16[8,33,1]{1,2,0:T(2,128)(2,1)S(1)} all-to-all(bf16[8,33,1]{1,2,0:T(2,128)(2,1)S(1)} %all_to_all.46), channel_id=1, replica_groups=mesh['ep'=8,'tp'=4] {'ep'}, dimensions={0} | all-to-all | bytes 1056 | tf_op jit(solution)/shard_map/all_to_all | solution.py:71
  61.6 0.1 reshape.94
  61.7 1.8 %fusion.3 = f32[264,256]{1,0:T(8,128)S(1)} fusion(bf16[264,2048]{1,0:T(8,128)(2,1)} %all-gather.3.cloned.1.call-done, bf16[1,2048,256]{2,1,0:T(8,128)(2,1)S(1)} %copy-done.3), kind=kOutput, calls=%fused_computation.11 | convolution fusion | flops 276824064 | bytes 2400256 | tf_op jit(solution)/shard_map/dot_general | solution.py:21
  63.5 0.5 fusion.9
  64.0 4.9 %all-gather.5.cloned.1.call-done = bf16[264,2048]{1,0:T(8,128)(2,1)} async-done(((bf16[264,512]{1,0:T(8,128)(2,1)}), bf16[264,2048]{1,0:T(8,128)(2,1)}) %all-gather.5.cloned.1.call-update) | async-done | bytes 1081360 | tf_op jit(solution)/shard_map/all_gather | solution.py:75
  68.9 2.2 %multiply_reduce_fusion = (f32[264]{0:T(512)S(1)}, f32[264,256]{1,0:T(8,128)S(1)}) fusion(f32[264,256]{1,0:T(8,128)S(1)} %fusion.3, f32[264,256]{1,0:T(8,128)S(1)} %fusion.9, bf16[264,2048]{1,0:T(8,128)(2,1)} %all-gather.5.cloned.1.call-done, bf16[1,256,2048]{2,1,0:T(8,128)(2,1)} %param.13), kind=kOutput, calls=%fused_computation.22 | convolution fusion | flops 277567232 | bytes 2941984 | tf_op jit(solution)/shard_map/dot_general | solution.py:27
  71.1 0.6 fusion.7
  71.7 1.6 %fusion = bf16[264,2048]{1,0:T(8,128)(2,1)} fusion(f32[264,2048]{1,0:T(8,128)S(1)} %fusion.7, bf16[1,2048,256]{2,1,0:T(8,128)(2,1)S(1)} %copy-done.3, f32[264,256]{1,0:T(8,128)S(1)} %fusion.3, f32[264,256]{1,0:T(8,128)S(1)} %get-tuple-element.14, f32[264]{0:T(512)S(1)} %reshape.94, f32[264,256]{1,0:T(8,128)S(1)} %fusion.9), kind=kOutput, calls=%fused_computation.7 | convolution fusion | flops 278716416 | bytes 5104672 | tf_op jit(solution)/shard_map/dot_general | solution.py:47
  73.3 5.9 %psum.7 = bf16[264]{0:T(512)(128)(2,1)S(1)} all-reduce(f32[264]{0:T(512)S(1)} %get-tuple-element.13), channel_id=1, replica_groups=mesh['ep'=8,'tp'=4] {'tp'}, use_global_device_ids=true, to_apply=%region_7.8 | all-reduce | flops 264 | bytes 1584 | tf_op jit(solution)/shard_map/psum | solution.py:83
  79.2 0.7 all_to_all.47
  79.9 5.7 %all-to-all-start.4 = ((bf16[8,33,1]{1,2,0:T(2,128)(2,1)}), bf16[8,33,1]{1,2,0:T(2,128)(2,1)S(1)}, u32[]{:S(2)}, u32[]{:S(2)}) async-start(bf16[8,33,1]{1,2,0:T(2,128)(2,1)} %all_to_all.47), calls=%async_computation.5 | async-start | bytes 8192 | tf_op jit(solution)/shard_map/all_to_all | solution.py:86
  85.6 12.9 %reduce-scatter.2.cloned.1.call-done = bf16[264,512]{1,0:T(8,128)(2,1)} async-done(((bf16[264,2048]{1,0:T(8,128)(2,1)}), bf16[264,512]{1,0:T(8,128)(2,1)}) %reduce-scatter.2.cloned.1.call-update) | async-done | bytes 270352 | tf_op jit(solution)/shard_map/reduce_scatter | solution.py:80
  98.5 1.8 %all_to_all.40 = bf16[8,33,512]{2,1,0:T(8,128)(2,1)} reshape(bf16[264,512]{1,0:T(8,128)(2,1)} %reduce-scatter.2.cloned.1.call-done) | data formatting | bytes 540672 | tf_op jit(solution)/shard_map/all_to_all | solution.py:85
  100.3 5.5 %all-to-all-start.3 = ((bf16[8,33,512]{2,1,0:T(8,128)(2,1)}), bf16[8,33,512]{2,1,0:T(8,128)(2,1)S(1)}, u32[]{:S(2)}, u32[]{:S(2)}) async-start(bf16[8,33,512]{2,1,0:T(8,128)(2,1)} %all_to_all.40), calls=%async_computation.4 | async-start | bytes 655360 | tf_op jit(solution)/shard_map/all_to_all | solution.py:85
  105.8 3.1 %fusion.1 = bf16[1,256,2048]{2,1,0:T(8,128)(2,1)} fusion(bf16[264,2048]{1,0:T(8,128)(2,1)} %all-gather.5.cloned.1.call-done, f32[264]{0:T(512)S(1)} %reshape.94, f32[264,256]{1,0:T(8,128)S(1)} %fusion.3, f32[264,256]{1,0:T(8,128)S(1)} %fusion.9), kind=kOutput, calls=%fused_computation.9 | convolution fusion | flops 278091776 | bytes 2671648 | tf_op jit(solution)/shard_map/dot_general | solution.py:41
  108.9 0.1 all_to_all.45
  109.0 1.9 %gather_fusion.4 = bf16[256]{0:T(256)(128)(2,1)S(1)} fusion(bf16[264]{0:T(512)(128)(2,1)S(1)} %all_to_all.45, s32[1024]{0:T(1024)S(1)} %pad_clamp_fusion), kind=kCustom, calls=%fused_computation.4 | custom fusion | bytes 2048 | tf_op jit(solution)/shard_map/gather | solution.py:92
  110.9 0.2 reshape.93
  111.1 0.6 copy.21
  111.7 4.3 %all-to-all-done.3 = bf16[8,33,512]{2,1,0:T(8,128)(2,1)S(1)} async-done(((bf16[8,33,512]{2,1,0:T(8,128)(2,1)}), bf16[8,33,512]{2,1,0:T(8,128)(2,1)S(1)}, u32[]{:S(2)}, u32[]{:S(2)}) %all-to-all-start.3) | async-done | bytes 270368 | tf_op jit(solution)/shard_map/all_to_all | solution.py:85
  115.9 0.1 all_to_all.42
  116.0 1.2 gather_fusion.3
  117.2 0.1 reshape.92
  117.3 1.3 %reduce_sum.34 = bf16[128,512]{1,0:T(8,128)(2,1)} reduce(bf16[128,2,512]{2,1,0:T(2,128)(2,1)S(1)} %reshape.92, bf16[]{:T(256)} %constant.37.clone.1), dimensions={1}, to_apply=%region_5.6 | reduce | flops 65536 | bytes 393218 | tf_op jit(solution)/shard_map/reduce_sum | solution.py:91
  (33 shorter events, 0.3 us)
Async XLA Ops:
  7.2 56.3 %copy-start = (bf16[1,2048,256]{2,1,0:T(8,128)(2,1)S(1)}, bf16[1,2048,256]{2,1,0:T(8,128)(2,1)}, u32[]{:S(2)}) copy-start(bf16[1,2048,256]{2,1,0:T(8,128)(2,1)} %param.11) | copy-start | bytes 3145732
  7.2 4.6 %copy-start.1 = (bf16[128,512]{1,0:T(8,128)(2,1)S(1)}, bf16[128,512]{1,0:T(8,128)(2,1)}, u32[]{:S(2)}) copy-start(bf16[128,512]{1,0:T(8,128)(2,1)} %param.7) | copy-start | bytes 393220
  7.2 54.5 %all-gather.3.cloned.1.call-start = ((), (), s32[]{:S(2)}) async-start(), calls=%async_computation.6 | async-start | bytes 1351680 | tf_op jit(solution)/shard_map/all_gather | solution.py:74
  11.8 2.1 %copy-start.2 = (bf16[128,512]{1,0:T(8,128)(2,1)S(1)}, bf16[128,512]{1,0:T(8,128)(2,1)}, u32[]{:S(2)}) copy-start(bf16[128,512]{1,0:T(8,128)(2,1)} %param.8) | copy-start | bytes 393220
  34.2 15.4 %copy-start.4 = (bf16[128,2]{0,1:T(2,128)(2,1)S(1)}, bf16[128,2]{0,1:T(2,128)(2,1)}, u32[]{:S(2)}) copy-start(bf16[128,2]{0,1:T(2,128)(2,1)} %param.10) | copy-start | bytes 1540
  35.0 34.0 %all-gather.5.cloned.1.call-start = ((), (), s32[]{:S(2)}) async-start(), calls=%async_computation.7 | async-start | bytes 1351680 | tf_op jit(solution)/shard_map/all_gather | solution.py:75
  48.7 13.0 %copy-start.3 = (bf16[1,2048,256]{2,1,0:T(8,128)(2,1)S(1)}, bf16[1,2048,256]{2,1,0:T(8,128)(2,1)}, u32[]{:S(2)}) copy-start(bf16[1,2048,256]{2,1,0:T(8,128)(2,1)} %param.12) | copy-start | bytes 3145732
  49.5 49.0 %reduce-scatter.2.cloned.1.call-start = ((), (), s32[]{:S(2)}) async-start(), calls=%async_computation.8 | async-start | bytes 1351680 | tf_op jit(solution)/shard_map/reduce_scatter | solution.py:80
  61.7 1.8 %copy-start.5 = (bf16[264,2048]{1,0:T(8,128)(2,1)S(1)}, bf16[264,2048]{1,0:T(8,128)(2,1)}, u32[]{:S(2)}) copy-start(bf16[264,2048]{1,0:T(8,128)(2,1)} %all-gather.3.cloned.1.call-done) | copy-start | bytes 3244036
  79.9 20.4 %all-to-all-start.4 = ((bf16[8,33,1]{1,2,0:T(2,128)(2,1)}), bf16[8,33,1]{1,2,0:T(2,128)(2,1)S(1)}, u32[]{:S(2)}, u32[]{:S(2)}) async-start(bf16[8,33,1]{1,2,0:T(2,128)(2,1)} %all_to_all.47), calls=%async_computation.5 | async-start | bytes 8192 | tf_op jit(solution)/shard_map/all_to_all | solution.py:86
  100.3 15.7 %all-to-all-start.3 = ((bf16[8,33,512]{2,1,0:T(8,128)(2,1)}), bf16[8,33,512]{2,1,0:T(8,128)(2,1)S(1)}, u32[]{:S(2)}, u32[]{:S(2)}) async-start(bf16[8,33,512]{2,1,0:T(8,128)(2,1)} %all_to_all.40), calls=%async_computation.4 | async-start | bytes 655360 | tf_op jit(solution)/shard_map/all_to_all | solution.py:85
Sparse Core Ops, SparseCore 0:
  35.1 15.3 all-gather.2
  52.0 16.8 all-gather.4
  73.4 24.9 reduce-scatter.1
where the time goes:
time: 126 us; the launch traced here: 125 us
  blocking collectives  46.7 us (37%)
  waiting for transfers between devices  22.2 us (18%)
  local copies, waits for them, and re-layouts  18.3 us (15%)
  between operations  14 us (11%)
  starting transfers between devices  11.3 us (9%)
  matrix products  9.68 us (8%)
  other arithmetic  2.92 us (2%)
    all_to_all x1, blocking collectives, per_device(): lax.all_to_all(send_rows, 'ep', split_axis=0, concat_axis=0, tiled=True)  18 us
    all_to_all x1, blocking collectives, per_device(): lax.all_to_all(send_grads, 'ep', split_axis=0, concat_axis=0, tiled=True)  13.6 us
    reduce_scatter x1, waiting for transfers between devices, per_device(): lax.psum_scatter(token_part.astype(jnp.bfloat16), 'tp', scatter_dimension...  12.9 us
    all_to_all x1, blocking collectives, per_device(): lax.all_to_all(send_scales, 'ep', split_axis=0, concat_axis=0, tiled=True)  9.24 us
    psum x1, blocking collectives, per_device(): score_total = lax.psum(scores, 'tp')  5.89 us
    all_to_all x1, starting transfers between devices, per_device(): lax.all_to_all(score_total.astype(jnp.bfloat16), 'ep', split_axis=0, conc...  5.66 us
    all_to_all x1, starting transfers between devices, per_device(): lax.all_to_all(token_share, 'ep', split_axis=0, concat_axis=0, tiled=True)  5.51 us
    all_gather x1, waiting for transfers between devices, per_device(): lax.all_gather(part_grads, 'tp', axis=1, tiled=True)  4.95 us
  transfers between devices with their start and end apart: 5, of which 3 were waited for; matrix products, arithmetic and copies ran while one was open for 9% of the time, Pallas kernels for 0%

commit v1 on v0

--- a/solution.py
+++ b/solution.py
@@ -1,10 +1,15 @@
+import functools
+
 import jax
 import jax.numpy as jnp
 from jax import lax
+from jax.experimental import pallas as pl
+from jax.experimental.pallas import tpu as pltpu
 from jax.sharding import PartitionSpec as P
 
 clamp_limit = 7.0
 alpha_gate = 1.702
+GROUPS = 1
 
 
 def ranks_within(route_block, experts):
@@ -50,7 +55,7 @@
     return (token_part, scores, down_part)
 
 
-def per_device(tokens, cotangent, routes, route_weights, gate_weight, up_weight, down_weight):
+def native(tokens, cotangent, routes, route_weights, gate_weight, up_weight, down_weight):
     experts = lax.axis_size("ep")
     tok_rows, top_count = routes.shape
     slots_each = tok_rows * top_count // experts + 1
@@ -93,6 +98,444 @@
     return (token_grad, weight_grad, down_part.astype(jnp.bfloat16)[None])
 
 
+def xor_index(value, mask):
+    bit = 1
+    while bit <= mask:
+        if mask & bit:
+            value = value + bit - 2 * bit * ((value // bit) % 2)
+        bit *= 2
+    return value
+
+
+def dot_nn(a, b):
+    return lax.dot_general(a, b, (((1,), (0,)), ((), ())), preferred_element_type=jnp.float32)
+
+
+def dot_nt(a, b):
+    return lax.dot_general(a, b, (((1,), (1,)), ((), ())), preferred_element_type=jnp.float32)
+
+
+def dot_tn(a, b):
+    return lax.dot_general(a, b, (((0,), (0,)), ((), ())), preferred_element_type=jnp.float32)
+
+
+def fused_kernel(
+    peers, main, spare, spare_rows, groups,
+    tokens_ref, cotangent_ref, routes_ref, scale_ref, gate_hbm, up_hbm, down_hbm,
+    token_out, weight_out, down_out,
+    gate_v, up_v, down_v, send_main, send_spare, rows_all, spare_all,
+    part, core_part, y_send, y_part, ret_send, ret_recv, ret_spare_send, ret_spare_recv,
+    score_own, score_core, score_sum, score_y, score_send, score_recv, weighted_v, down_stage,
+    w_sem, down_sem,
+    disp_s, disp_r, disp_es, disp_er, y_s, y_r, y_es, y_er,
+    core_s, core_r, core_es, core_er,
+    rs_s, rs_r, ry_s, ry_r, sc_s, sc_r, sy_s, sy_r,
+    ret_s, ret_r, ret_es, ret_er, ret_ss, ret_sr,
+):
+    f32, bf16 = jnp.float32, jnp.bfloat16
+    ep = lax.axis_index("ep")
+    tp = lax.axis_index("tp")
+    yy, cc = tp // 2, tp % 2
+    core_dev = {"tp": yy * 2 + 1 - cc}
+    y_dev = {"tp": (1 - yy) * 2 + cc}
+    other_y = 1 - yy
+
+    def ep_dev(m):
+        return {"ep": xor_index(ep, m)}
+
+    barrier = pltpu.get_barrier_semaphore()
+    devices = [ep_dev(m) for m in range(1, peers)] + [core_dev, y_dev]
+    for device in devices:
+        pl.semaphore_signal(
+            barrier, inc=1, device_id=device, device_id_type=pl.DeviceIdType.MESH
+        )
+    loads = [
+        pltpu.make_async_copy(gate_hbm.at[0], gate_v, w_sem.at[0]),
+        pltpu.make_async_copy(up_hbm.at[0], up_v, w_sem.at[1]),
+        pltpu.make_async_copy(down_hbm.at[0], down_v, w_sem.at[2]),
+    ]
+    for load in loads:
+        load.start()
+
+    tok = tokens_ref.shape[0]
+    width = tokens_ref.shape[1]
+    slots = peers * main + spare_rows
+    lanes = 128
+
+    def lane_iota(shape, dim):
+        return lax.broadcasted_iota(jnp.int32, shape, dim)
+
+    m_row = lane_iota((1, lanes), 1)
+    e_row = jnp.zeros((1, lanes), jnp.int32)
+    bit = 1
+    while bit < peers:
+        mine = (ep // bit) % 2
+        have = jnp.where((m_row & bit) != 0, 1, 0)
+        e_row = e_row + bit * (have + mine - 2 * have * mine)
+        bit *= 2
+    e_row = jnp.where(m_row < peers, e_row, -1)
+    first = (routes_ref[:, 0:1] == e_row).astype(f32)
+    second = (routes_ref[:, 1:2] == e_row).astype(f32)
+    named = first + second
+    tri = (lane_iota((tok, tok), 0) >= lane_iota((tok, tok), 1)).astype(bf16)
+    rank1 = named * dot_nn(tri, named.astype(bf16))
+    scale = scale_ref[...].astype(f32)
+    scale_m = first * scale[:, 0:1] + second * scale[:, 1:2]
+
+    s_mat = lane_iota((lanes, slots), 1)
+    m_mat = lane_iota((lanes, slots), 0)
+    base = peers * main
+    in_main = (s_mat < base) & (s_mat >= m_mat * main) & (s_mat < m_mat * main + main)
+    j_mat = s_mat - base
+    in_spare = (j_mat >= m_mat * spare) & (j_mat < m_mat * spare + spare) & (j_mat < peers * spare) & (j_mat >= 0)
+    expand = (in_main | in_spare).astype(f32).astype(bf16)
+    s_row = lane_iota((1, slots), 1)
+    t_main = s_row + 1
+    t_spare = s_row - base + 1 + main
+    for m in range(1, peers):
+        t_main = t_main - jnp.where(s_row >= m * main, main, 0)
+        t_spare = t_spare - jnp.where(s_row - base >= m * spare, spare, 0)
+    target = jnp.where(s_row < base, t_main, jnp.where(s_row < base + peers * spare, t_spare, -5))
+    ranks_s = dot_nn(rank1.astype(bf16), expand)
+    pick = (ranks_s == target.astype(f32)).astype(f32).astype(bf16)
+
+    x_slots = dot_tn(pick, tokens_ref[...])
+    g_slots = dot_tn(pick, cotangent_ref[...])
+    x_main = x_slots[:base].astype(bf16).reshape(peers, main, width)
+    g_main = g_slots[:base].astype(bf16).reshape(peers, main, width)
+    send_main[0] = x_main
+    send_main[1] = g_main
+    rows_all[0, tp, 0] = x_main[0]
+    rows_all[1, tp, 0] = g_main[0]
+    lane1 = (lane_iota((tok, lanes), 1) + 1).astype(f32)
+    spare_h = 2 * spare + 1
+    row_id = lane_iota((spare_h, width), 0)
+    for m in range(peers):
+        w_row = jnp.sum(
+            jnp.where(rank1[:, m : m + 1] == lane1, scale_m[:, m : m + 1], 0.0), axis=0, keepdims=True
+        )
+        wide = jnp.concatenate([w_row, jnp.zeros((1, width - lanes), f32)], axis=1)
+        block = jnp.broadcast_to(wide, (spare_h, width))
+        for x in range(spare):
+            j = base + m * spare + x
+            block = jnp.where(row_id == x, x_slots[j : j + 1], block)
+            block = jnp.where(row_id == spare + x, g_slots[j : j + 1], block)
+        block = block.astype(bf16)
+        send_spare[m] = block
+        if m == 0:
+            spare_all[tp, 0] = block
+
+    pl.semaphore_wait(barrier, len(devices))
+
+    pending = []
+
+    def remote(src, dst, s_sem, r_sem, device):
+        copy = pltpu.make_async_remote_copy(
+            src_ref=src, dst_ref=dst, send_sem=s_sem, recv_sem=r_sem,
+            device_id=device, device_id_type=pl.DeviceIdType.MESH,
+        )
+        copy.start()
+        pending.append(copy)
+        return copy
+
+    disp = {}
+
+    def dispatch(m):
+        disp[m] = (
+            remote(send_spare.at[m], spare_all.at[tp, m], disp_es.at[m], disp_er.at[m], ep_dev(m)),
+            remote(send_main.at[:, m], rows_all.at[:, tp, m], disp_s.at[m], disp_r.at[m], ep_dev(m)),
+        )
+
+    y_copy, core_a, core_b = {}, {}, {}
+
+    def forward(m):
+        if m > 0:
+            for copy in disp[m]:
+                copy.wait_recv()
+        if m > 0:
+            src, src_e = rows_all.at[:, tp, m], spare_all.at[tp, m]
+        else:
+            src, src_e = send_main.at[:, 0], send_spare.at[0]
+        dst, dst_e = rows_all.at[:, tp, m], spare_all.at[tp, m]
+        y_copy[m] = (
+            remote(src_e, dst_e, y_es.at[m], y_er.at[m], y_dev),
+            remote(src, dst, y_s.at[m], y_r.at[m], y_dev),
+        )
+        core_a[m] = (
+            remote(src_e, dst_e, core_es.at[0, m], core_er.at[0, m], core_dev),
+            remote(src, dst, core_s.at[0, m], core_r.at[0, m], core_dev),
+        )
+
+    y_tp = other_y * 2 + cc
+
+    def relay(m):
+        for copy in y_copy[m]:
+            copy.wait_recv()
+        core_b[m] = (
+            remote(spare_all.at[y_tp, m], spare_all.at[y_tp, m], core_es.at[1, m], core_er.at[1, m], core_dev),
+            remote(rows_all.at[:, y_tp, m], rows_all.at[:, y_tp, m], core_s.at[1, m], core_r.at[1, m], core_dev),
+        )
+
+    def settle(m):
+        for copy in core_a[m] + core_b[m]:
+            copy.wait_recv()
+
+    tp_size = rows_all.shape[1]
+    eye = (lane_iota((main, lanes), 0) == lane_iota((main, lanes), 1))
+    spare_row = lane_iota((spare_rows, 1), 0)
+    wide_row = lane_iota((spare_rows, width), 0)
+    lane_row = lane_iota((1, lanes), 1)
+
+    def spare_tile(which, t):
+        tile = jnp.zeros((spare_rows, width), f32)
+        for m in range(peers):
+            block = spare_all[t, m].astype(f32)
+            for x in range(spare):
+                row = which * spare + x
+                tile = jnp.where(wide_row == m * spare + x, block[row : row + 1], tile)
+        return tile.astype(bf16)
+
+    spans = [(g * peers // groups, (g + 1) * peers // groups) for g in range(groups)]
+
+    def rows_of(which, t, lo, hi):
+        block = rows_all[which, t, lo:hi].reshape((hi - lo) * main, width)
+        if hi == peers:
+            block = jnp.concatenate([block, spare_tile(which, t)], axis=0)
+        return block
+
+    rs_copy, ry_copy, small = {}, {}, {}
+
+    def compute(g):
+        lo, hi = spans[g]
+        last = hi == peers
+        gate_pre = up_pre = back = None
+        for t in range(tp_size):
+            x_t = rows_of(0, t, lo, hi)
+            g_t = rows_of(1, t, lo, hi)
+            terms = (
+                dot_nn(x_t, gate_v[t * width : (t + 1) * width, :]),
+                dot_nn(x_t, up_v[t * width : (t + 1) * width, :]),
+                dot_nt(g_t, down_v[:, t * width : (t + 1) * width]),
+            )
+            if t == 0:
+                gate_pre, up_pre, back = terms
+            else:
+                gate_pre, up_pre, back = gate_pre + terms[0], up_pre + terms[1], back + terms[2]
+        cols = []
+        spare_col = jnp.zeros((spare_rows, 1), f32)
+        for m in range(peers):
+            w_row = spare_all[0, m].astype(f32)[2 * spare : 2 * spare + 1, 0:lanes]
+            if lo <= m < hi:
+                cols.append(jnp.sum(jnp.where(eye, w_row, 0.0), axis=1, keepdims=True))
+            if last:
+                for x in range(spare):
+                    spare_col = jnp.where(
+                        spare_row == m * spare + x, w_row[:, main + x : main + x + 1], spare_col
+                    )
+        if last:
+            cols.append(spare_col)
+        weight_col = jnp.concatenate(cols, axis=0)
+        gate_clip = jnp.minimum(gate_pre, clamp_limit)
+        up_clip = jnp.clip(up_pre, -clamp_limit, clamp_limit)
+        sigmoid_gate = jax.nn.sigmoid(alpha_gate * gate_clip)
+        swish_gate = gate_clip * sigmoid_gate
+        hidden = (up_clip + 1.0) * swish_gate
+        scores = jnp.sum(hidden * back, axis=1, keepdims=True)
+        scaled = back * weight_col
+        slope = sigmoid_gate + alpha_gate * swish_gate * (1.0 - sigmoid_gate)
+        gate_grad = jnp.where(gate_pre < clamp_limit, scaled * (up_clip + 1.0) * slope, 0.0).astype(bf16)
+        up_grad = jnp.where(jnp.abs(up_pre) < clamp_limit, scaled * swish_gate, 0.0).astype(bf16)
+        row_lo, row_n = lo * main, gate_pre.shape[0]
+        weighted_v[row_lo : row_lo + row_n, :] = (hidden * weight_col).astype(bf16)
+        for m in range(lo, hi):
+            col = scores[(m - lo) * main : (m - lo + 1) * main]
+            score_own[m] = jnp.sum(jnp.where(eye, col, 0.0), axis=0, keepdims=True)
+        if last:
+            for m in range(peers):
+                row = score_own[m]
+                for x in range(spare):
+                    j = (hi - lo) * main + m * spare + x
+                    row = jnp.where(lane_row == main + x, scores[j : j + 1], row)
+                score_own[m] = row
+            small[0] = remote(score_own, score_core, sc_s, sc_r, core_dev)
+        for t in range(tp_size):
+            term = dot_nt(gate_grad, gate_v[t * width : (t + 1) * width, :])
+            term = term + dot_nt(up_grad, up_v[t * width : (t + 1) * width, :])
+            part[t // 2, t % 2, row_lo : row_lo + row_n, :] = term.astype(bf16)
+        rows = pl.ds(row_lo, row_n)
+        rs_copy[g] = remote(
+            part.at[:, 1 - cc, rows], core_part.at[:, rows], rs_s.at[g], rs_r.at[g], core_dev
+        )
+
+    def span_rows(g):
+        lo, hi = spans[g]
+        return lo * main, (hi - lo) * main + (spare_rows if hi == peers else 0)
+
+    def reduce_core(g):
+        row_lo, row_n = span_rows(g)
+        rows = pl.ds(row_lo, row_n)
+        rs_copy[g].wait_recv()
+        y_send[rows, :] = (
+            part[other_y, cc, rows, :].astype(f32) + core_part[other_y, rows, :].astype(f32)
+        ).astype(bf16)
+        ry_copy[g] = remote(y_send.at[rows], y_part.at[rows], ry_s.at[g], ry_r.at[g], y_dev)
+        if spans[g][1] == peers:
+            small[0].wait_recv()
+            score_sum[...] = score_own[...] + score_core[...]
+            small[1] = remote(score_sum, score_y, sy_s, sy_r, y_dev)
+
+    returns = {}
+
+    def reduce_y(g):
+        lo, hi = spans[g]
+        row_lo, row_n = span_rows(g)
+        rows = pl.ds(row_lo, row_n)
+        ry_copy[g].wait_recv()
+        total = (
+            part[yy, cc, rows, :].astype(f32)
+            + core_part[yy, rows, :].astype(f32)
+            + y_part[rows, :].astype(f32)
+        )
+        ret_send[lo:hi] = total[: (hi - lo) * main].astype(bf16).reshape(hi - lo, main, width)
+        returns[g] = []
+        for m in range(max(lo, 1), hi):
+            returns[g].append(remote(ret_send.at[m], ret_recv.at[m], ret_s.at[m], ret_r.at[m], ep_dev(m)))
+        if hi == peers:
+            small[1].wait_recv()
+            score_send[...] = score_sum[...] + score_y[...]
+            for m in range(peers):
+                for x in range(spare):
+                    j = (hi - lo) * main + m * spare + x
+                    ret_spare_send[m, x : x + 1] = total[j : j + 1]
+            for m in range(1, peers):
+                returns[g].append(
+                    remote(ret_spare_send.at[m], ret_spare_recv.at[m], ret_es.at[m], ret_er.at[m], ep_dev(m))
+                )
+                returns[g].append(
+                    remote(score_send.at[m], score_recv.at[m], ret_ss.at[m], ret_sr.at[m], ep_dev(m))
+                )
+
+    for m in range(1, peers):
+        dispatch(m)
+    done = 0
+    for g, (lo, hi) in enumerate(spans):
+        for m in range(lo, hi):
+            forward(m)
+            if m > lo:
+                relay(m - 1)
+        relay(hi - 1)
+        if g == 0:
+            for load in loads:
+                load.wait()
+        if g > 0:
+            reduce_core(g - 1)
+        for m in range(lo, hi):
+            settle(m)
+        compute(g)
+        if g > 0:
+            reduce_y(g - 1)
+    reduce_core(groups - 1)
+    stores = []
+    half = tp_size // 2
+    def down_piece(t):
+        g_t = rows_of(1, t, 0, peers)
+        down_stage[:, t * width : (t + 1) * width] = dot_tn(weighted_v[...], g_t).astype(bf16)
+
+    for t in range(half):
+        down_piece(t)
+    reduce_y(groups - 1)
+    for t in range(half, tp_size):
+        down_piece(t)
+    store = pltpu.make_async_copy(down_stage, down_out.at[0], down_sem)
+    store.start()
+
+    for g in range(groups):
+        for copy in returns[g]:
+            copy.wait_recv()
+    back_rows = [ret_send[0]] + [ret_recv[m] for m in range(1, peers)]
+    tile = jnp.zeros((spare_rows, width), f32)
+    pair0 = jnp.zeros((tok, lanes), f32)
+    pair1 = jnp.zeros((tok, lanes), f32)
+    for m in range(peers):
+        block = ret_spare_send[0] if m == 0 else ret_spare_recv[m]
+        for x in range(spare):
+            tile = jnp.where(wide_row == m * spare + x, block[x : x + 1], tile)
+        row = score_send[0] if m == 0 else score_recv[m]
+        found = jnp.where(rank1[:, m : m + 1] == lane1, row, 0.0)
+        pair0 = pair0 + first[:, m : m + 1] * found
+        pair1 = pair1 + second[:, m : m + 1] * found
+    back_all = jnp.concatenate(back_rows + [tile.astype(bf16)], axis=0)
+    token_out[...] = dot_nn(pick, back_all).astype(bf16)
+    col0 = jnp.sum(pair0, axis=1, keepdims=True)
+    col1 = jnp.sum(pair1, axis=1, keepdims=True)
+    two = lane_iota((tok, 2), 1)
+    weight_out[...] = jnp.where(two == 0, col0, col1).astype(bf16)
+    for copy in pending:
+        copy.wait_send()
+    store.wait()
+
+
+def fused(tokens, cotangent, routes, route_weights, gate_weight, up_weight, down_weight):
+    peers = lax.axis_size("ep")
+    tp_size = lax.axis_size("tp")
+    tok, top_count = routes.shape
+    width = tokens.shape[1]
+    cap = tok * top_count // peers + 1
+    main = cap // 16 * 16
+    spare = cap - main
+    spare_rows = -(-(peers * spare) // 16) * 16
+    groups = GROUPS
+    total = peers * main + spare_rows
+    hid, full = down_weight.shape[1], down_weight.shape[2]
+    bf16, f32 = jnp.bfloat16, jnp.float32
+    vm = pltpu.VMEM
+    dma = pltpu.SemaphoreType.DMA
+    any_spec = pl.BlockSpec(memory_space=pl.ANY)
+    v_spec = pl.BlockSpec(memory_space=pltpu.VMEM)
+    spare_h = 2 * spare + 1
+    return pl.pallas_call(
+        functools.partial(fused_kernel, peers, main, spare, spare_rows, groups),
+        out_shape=(
+            jax.ShapeDtypeStruct((tok, width), bf16),
+            jax.ShapeDtypeStruct((tok, top_count), bf16),
+            jax.ShapeDtypeStruct((1, hid, full), bf16),
+        ),
+        in_specs=[v_spec] * 4 + [any_spec] * 3,
+        out_specs=(v_spec, v_spec, any_spec),
+        scratch_shapes=[
+            vm((full, hid), bf16), vm((full, hid), bf16), vm((hid, full), bf16),
+            vm((2, peers, main, width), bf16), vm((peers, spare_h, width), bf16),
+            vm((2, tp_size, peers, main, width), bf16), vm((tp_size, peers, spare_h, width), bf16),
+            vm((2, 2, total, width), bf16), vm((2, total, width), bf16),
+            vm((total, width), bf16), vm((total, width), bf16),
+            vm((peers, main, width), bf16), vm((peers, main, width), bf16),
+            vm((peers, spare, width), f32), vm((peers, spare, width), f32),
+            vm((peers, 1, 128), f32), vm((peers, 1, 128), f32), vm((peers, 1, 128), f32),
+            vm((peers, 1, 128), f32), vm((peers, 1, 128), f32), vm((peers, 1, 128), f32),
+            vm((total, hid), bf16), vm((hid, full), bf16),
+            dma((3,)), dma,
+        ]
+        + [dma((peers,))] * 8
+        + [dma((2, peers))] * 4
+        + [dma((groups,))] * 4
+        + [dma] * 4
+        + [dma((peers,))] * 6,
+        compiler_params=pltpu.CompilerParams(
+            collective_id=0, has_side_effects=True
+        ),
+    )(tokens, cotangent, routes, route_weights, gate_weight, up_weight, down_weight)
+
+
+def per_device(tokens, cotangent, routes, route_weights, gate_weight, up_weight, down_weight):
+    args = (tokens, cotangent, routes, route_weights, gate_weight, up_weight, down_weight)
+    cap = routes.shape[0] * routes.shape[1] // lax.axis_size("ep") + 1
+    peers = lax.axis_size("ep")
+    small = cap < 16 or cap % 16 == 0 or cap > 127 or peers & (peers - 1) != 0
+    if small or lax.axis_size("tp") != 4 or routes.shape[1] != 2:
+        return native(*args)
+    return fused(*args)
+
+
 def solution(mesh):
     placed = (
         P("ep", "tp"),

time: 126 us -> 56.3 us (0.45)
  Pallas kernels: 0 us -> 48 us
  blocking collectives: 46.7 us -> 0 us
  waiting for transfers between devices: 22.2 us -> 0 us
  between operations: 14 us -> 0.65 us
  starting transfers between devices: 11.3 us -> 0 us
  local copies, waits for them, and re-layouts: 18.3 us -> 7.35 us
  matrix products: 9.68 us -> 0 us
  other arithmetic: 2.92 us -> 0 us
    pallas_call x0 -> x1, Pallas kernels: none -> 48 us  [fused(): pl.pallas_call(functools.partial(fused_kernel, peers, main, spare, spare_...]
    all_to_all x3 -> x0, blocking collectives: 40.9 us -> none  [the longest x1 18 us: per_device(): lax.all_to_all(send_rows, 'ep', split_axis=0, concat_axis=0, tiled=True)]
    reduce_scatter x1 -> x0, waiting for transfers between devices: 12.9 us -> none  [per_device(): lax.psum_scatter(token_part.astype(jnp.bfloat16), 'tp', scatter_dimension...]
    all_to_all x2 -> x0, starting transfers between devices: 11.2 us -> none  [the longest x1 5.66 us: per_device(): lax.all_to_all(score_total.astype(jnp.bfloat16), 'ep', split_axis=0, conc...]
    dot_general x6 -> x0, matrix products: 9.68 us -> none  [the longest x1 3.07 us: expert_terms(): lax.dot_general(weighted, exp_grads, (((0,), (0,)), ((), ())), preferred_...]
    gather x7 -> x0, local copies, waits for them, and re-layouts: 9.63 us -> none  [the longest x1 2.37 us: per_device(): send_scales = jnp.where(filled, route_weights.reshape(-1)[pair_index], 0)]
    psum x1 -> x0, blocking collectives: 5.89 us -> none  [per_device(): score_total = lax.psum(scores, 'tp')]
    all_gather x2 -> x0, waiting for transfers between devices: 4.95 us -> none  [the longest x1 4.95 us: per_device(): lax.all_gather(part_grads, 'tp', axis=1, tiled=True)]
  transfers between devices with their start and end apart: 5 -> 0, of which waited for: 3 -> 0; matrix products, arithmetic and copies ran while one was open for 9% -> 0% of each run, Pallas kernels for 0% -> 0%
where the time goes in v1:
time: 56.3 us; the launch traced here: 56 us
  Pallas kernels  48 us (85%)
  local copies, waits for them, and re-layouts  7.35 us (13%)
  between operations  0.65 us (1%)
    pallas_call x1, Pallas kernels, fused(): pl.pallas_call(functools.partial(fused_kernel, peers, main, spare, spare_...  48 us
    unnamed x6, local copies, waits for them, and re-layouts  6 us
    pallas_call x1, local copies, waits for them, and re-layouts, fused(): pl.pallas_call(functools.partial(fused_kernel, peers, main, spare, spare_...  1.35 us

profile of v1, /device:TPU:0, one launch (start us, length us, event | category | flops | bytes accessed | tf_op | source)
XLA Modules:
  0.0 56.0 jit_solution(4831155340062351962)
XLA Ops:
  0.6 0.0 copy-start
  0.6 1.4 %copy.11.scale_ref = bf16[128,2]{1,0:T(8,128)(2,1)} copy(bf16[128,2]{0,1:T(2,128)(2,1)} %param.10) | data formatting | bytes 1024 | tf_op args[3]
  2.0 0.0 copy-done
  2.0 0.7 %copy.10.routes_ref = s32[128,2]{1,0:T(8,128)} copy(s32[128,2]{0,1:T(2,128)S(1)} %copy-done) | data formatting | bytes 2048 | tf_op args[2]
  2.8 48.0 %shard_map.94 = (bf16[128,512]{1,0:T(8,128)(2,1)}, bf16[128,2]{1,0:T(8,128)(2,1)}, bf16[1,256,2048]{2,1,0:T(8,128)(2,1)}) custom-call(bf16[128,512]{1,0:T(8,128)(2,1)} %tokens_ref.1, bf16[128,512]{1,0:T(8,128)(2,1)} %cotangent_ref.1, s32[128,2]{1,0:T(8,128)} %copy.10.routes_ref, bf16[128,2]{1,0:T(8,128)(2,1)} %copy.11.scale_ref, ...), custom_call_target="tpu_custom_call" | custom-call | tf_op jit(solution)/shard_map/pallas_call | solution.py:496
  50.8 1.4 %copy.12 = bf16[128,2]{0,1:T(2,128)(2,1)} copy(bf16[128,2]{1,0:T(8,128)(2,1)} %get-tuple-element.4) | data formatting | bytes 1024 | tf_op jit(solution)/shard_map/pallas_call | solution.py:496
  52.1 1.6 %copy.15 = bf16[128,512]{1,0:T(8,128)(2,1)} copy(bf16[128,512]{1,0:T(8,128)(2,1)} %get-tuple-element.9) | data formatting | bytes 262144
  53.7 2.3 %copy.16 = bf16[1,256,2048]{2,1,0:T(8,128)(2,1)} copy(bf16[1,256,2048]{2,1,0:T(8,128)(2,1)} %get-tuple-element.11) | data formatting | bytes 2097152
Async XLA Ops:
  0.6 1.4 %copy-start = (s32[128,2]{0,1:T(2,128)S(1)}, s32[128,2]{0,1:T(2,128)}, u32[]{:S(2)}) copy-start(s32[128,2]{0,1:T(2,128)} %param.9) | copy-start | bytes 3076

commit v2 on v0

--- a/solution.py
+++ b/solution.py
@@ -1,10 +1,16 @@
+import functools
+
 import jax
 import jax.numpy as jnp
 from jax import lax
+from jax.experimental import pallas as pl
+from jax.experimental.pallas import tpu as pltpu
 from jax.sharding import PartitionSpec as P
 
 clamp_limit = 7.0
 alpha_gate = 1.702
+send_order = (1, 2, 3, 4, 5, 6, 7)
+relay_lag = 4
 
 
 def ranks_within(route_block, experts):
@@ -50,7 +56,7 @@
     return (token_part, scores, down_part)
 
 
-def per_device(tokens, cotangent, routes, route_weights, gate_weight, up_weight, down_weight):
+def native(tokens, cotangent, routes, route_weights, gate_weight, up_weight, down_weight):
     experts = lax.axis_size("ep")
     tok_rows, top_count = routes.shape
     slots_each = tok_rows * top_count // experts + 1
@@ -93,6 +99,407 @@
     return (token_grad, weight_grad, down_part.astype(jnp.bfloat16)[None])
 
 
+def xor_index(value, mask):
+    bit = 1
+    while bit <= mask:
+        if mask & bit:
+            value = value + bit - 2 * bit * ((value // bit) % 2)
+        bit *= 2
+    return value
+
+
+def dot_nn(a, b):
+    return lax.dot_general(a, b, (((1,), (0,)), ((), ())), preferred_element_type=jnp.float32)
+
+
+def dot_nt(a, b):
+    return lax.dot_general(a, b, (((1,), (1,)), ((), ())), preferred_element_type=jnp.float32)
+
+
+def dot_tn(a, b):
+    return lax.dot_general(a, b, (((0,), (0,)), ((), ())), preferred_element_type=jnp.float32)
+
+
+def fused_kernel(
+    peers, main, spare, spare_rows, order, chunks,
+    tokens_ref, cotangent_ref, routes_ref, scale_ref, gate_hbm, up_hbm, down_hbm,
+    token_out, weight_out, down_out,
+    gate_v, up_v, down_v, send_main, send_spare, rows_all, spare_all,
+    part, core_part, y_send, y_part, ret_send, ret_recv, ret_spare_send, ret_spare_recv,
+    score_own, score_core, score_sum, score_y, score_send, score_recv, weighted_v,
+    w_sem, disp_s, disp_r, disp_es, disp_er, y_s, y_r, y_es, y_er,
+    core_s, core_r, core_es, core_er,
+    rs_s, rs_r, ry_s, ry_r, sc_s, sc_r, sy_s, sy_r,
+    ret_s, ret_r, ret_es, ret_er, ret_ss, ret_sr,
+):
+    f32, bf16 = jnp.float32, jnp.bfloat16
+    ep = lax.axis_index("ep")
+    tp = lax.axis_index("tp")
+    yy, cc = tp // 2, tp % 2
+    other_y, other_c = 1 - yy, 1 - cc
+    core_tp, y_tp, far_tp = yy * 2 + other_c, other_y * 2 + cc, other_y * 2 + other_c
+    core_dev, y_dev = {"tp": core_tp}, {"tp": y_tp}
+
+    def ep_dev(m):
+        return {"ep": xor_index(ep, m)}
+
+    barrier = pltpu.get_barrier_semaphore()
+    devices = [ep_dev(m) for m in range(1, peers)] + [core_dev, y_dev]
+    for device in devices:
+        pl.semaphore_signal(
+            barrier, inc=1, device_id=device, device_id_type=pl.DeviceIdType.MESH
+        )
+    loads = [
+        pltpu.make_async_copy(gate_hbm.at[0], gate_v, w_sem.at[0]),
+        pltpu.make_async_copy(up_hbm.at[0], up_v, w_sem.at[1]),
+        pltpu.make_async_copy(down_hbm.at[0], down_v, w_sem.at[2]),
+    ]
+    for load in loads:
+        load.start()
+
+    tok, width = tokens_ref.shape
+    base = peers * main
+    slots = base + spare_rows
+    padded = score_own.shape[1]
+    group = 16
+
+    def iota(shape, dim):
+        return lax.broadcasted_iota(jnp.int32, shape, dim)
+
+    m_col = iota((group, 1), 0)
+    e_col = jnp.zeros((group, 1), jnp.int32)
+    bit = 1
+    while bit < peers:
+        mine = (ep // bit) % 2
+        have = jnp.where((m_col & bit) != 0, 1, 0)
+        e_col = e_col + bit * (have + mine - 2 * have * mine)
+        bit *= 2
+    e_col = jnp.where(m_col < peers, e_col, -1)
+    first = (routes_ref[0:1, :] == e_col).astype(f32)
+    second = (routes_ref[1:2, :] == e_col).astype(f32)
+    named = first + second
+    tri = (iota((tok, tok), 0) <= iota((tok, tok), 1)).astype(f32).astype(bf16)
+    rank1 = named * dot_nn(named.astype(bf16), tri)
+    scale = scale_ref[...].astype(f32)
+    scale_m = (first * scale[0:1, :] + second * scale[1:2, :]).astype(bf16)
+
+    def in_block(place, m):
+        in_main = (place >= m * main) & (place < m * main + main)
+        low = base + m * spare
+        return in_main | ((place >= low) & (place < low + spare))
+
+    expand = in_block(iota((slots, group), 0), iota((slots, group), 1))
+    expand = (expand & (iota((slots, group), 1) < peers)).astype(f32).astype(bf16)
+    s_col = iota((slots, 1), 0)
+    t_main = s_col + 1
+    t_spare = s_col - base + 1 + main
+    for m in range(1, peers):
+        t_main = t_main - jnp.where(s_col >= m * main, main, 0)
+        t_spare = t_spare - jnp.where(s_col - base >= m * spare, spare, 0)
+    target = jnp.where(s_col < base, t_main, jnp.where(s_col < base + peers * spare, t_spare, -5))
+    ranks_s = dot_nn(expand, rank1.astype(bf16))
+    pick = (ranks_s == target.astype(f32)).astype(f32).astype(bf16)
+    pick_pad = jnp.concatenate([pick, jnp.zeros((padded - slots, tok), bf16)], axis=0)
+
+    x_slots = dot_nn(pick, tokens_ref[...])
+    x_main = x_slots[:base].astype(bf16).reshape(peers, main, width)
+    send_main[0] = x_main
+    rows_all[0, tp, 0] = x_main[0]
+    g_slots = dot_nn(pick, cotangent_ref[...])
+    g_main = g_slots[:base].astype(bf16).reshape(peers, main, width)
+    send_main[1] = g_main
+    rows_all[1, tp, 0] = g_main[0]
+    w_rows = dot_nt(scale_m, pick_pad)
+    w_rows = jnp.concatenate([w_rows, jnp.zeros((group, width - padded), f32)], axis=1)
+    spare_h = 2 * spare + 1
+    row_id = iota((spare_h, width), 0)
+    for m in range(peers):
+        block = jnp.broadcast_to(w_rows[m : m + 1], (spare_h, width))
+        for x in range(spare):
+            j = base + m * spare + x
+            block = jnp.where(row_id == x, x_slots[j : j + 1], block)
+            block = jnp.where(row_id == spare + x, g_slots[j : j + 1], block)
+        block = block.astype(bf16)
+        send_spare[m] = block
+        if m == 0:
+            spare_all[tp, 0] = block
+
+    pl.semaphore_wait(barrier, len(devices))
+
+    pending = []
+
+    def remote(src, dst, s_sem, r_sem, device):
+        copy = pltpu.make_async_remote_copy(
+            src_ref=src, dst_ref=dst, send_sem=s_sem, recv_sem=r_sem,
+            device_id=device, device_id_type=pl.DeviceIdType.MESH,
+        )
+        copy.start()
+        pending.append(copy)
+        return copy
+
+    disp, y_copy, core_a, core_b = {}, {}, {}, {}
+
+    def dispatch(w, m):
+        disp[w, m] = [
+            remote(send_main.at[w, m], rows_all.at[w, tp, m], disp_s.at[w, m], disp_r.at[w, m], ep_dev(m))
+        ]
+        if w == 0:
+            disp[w, m].append(
+                remote(send_spare.at[m], spare_all.at[tp, m], disp_es.at[m], disp_er.at[m], ep_dev(m))
+            )
+
+    def forward(w, m):
+        if m > 0:
+            for copy in disp[w, m]:
+                copy.wait_recv()
+        src = rows_all.at[w, tp, m] if m > 0 else send_main.at[w, 0]
+        dst = rows_all.at[w, tp, m]
+        y_copy[w, m] = [remote(src, dst, y_s.at[w, m], y_r.at[w, m], y_dev)]
+        core_a[w, m] = [remote(src, dst, core_s.at[0, w, m], core_r.at[0, w, m], core_dev)]
+        if w == 0:
+            src = spare_all.at[tp, m] if m > 0 else send_spare.at[0]
+            dst = spare_all.at[tp, m]
+            y_copy[w, m].append(remote(src, dst, y_es.at[m], y_er.at[m], y_dev))
+            core_a[w, m].append(remote(src, dst, core_es.at[0, m], core_er.at[0, m], core_dev))
+
+    def relay(w, m):
+        for copy in y_copy[w, m]:
+            copy.wait_recv()
+        block = rows_all.at[w, y_tp, m]
+        core_b[w, m] = [remote(block, block, core_s.at[1, w, m], core_r.at[1, w, m], core_dev)]
+        if w == 0:
+            block = spare_all.at[y_tp, m]
+            core_b[w, m].append(remote(block, block, core_es.at[1, m], core_er.at[1, m], core_dev))
+
+    def settle(copies, w):
+        for m in range(peers):
+            for copy in copies[w, m]:
+                copy.wait_recv()
+
+    tp_size = rows_all.shape[1]
+    wide_row = iota((spare_rows, width), 0)
+
+    def spare_tile(which, t):
+        tile = jnp.zeros((spare_rows, width), f32)
+        for m in range(peers):
+            block = spare_all[t, m].astype(f32)
+            for x in range(spare):
+                row = which * spare + x
+                tile = jnp.where(wide_row == m * spare + x, block[row : row + 1], tile)
+        return tile.astype(bf16)
+
+    def rows_of(which, t):
+        block = rows_all[which, t].reshape(base, width)
+        return jnp.concatenate([block, spare_tile(which, t)], axis=0)
+
+    def cut(t):
+        return pl.ds(pl.multiple_of(t * width, width), width)
+
+    for m in order:
+        dispatch(0, m)
+    for m in order:
+        dispatch(1, m)
+    turn = (0,) + order
+    items = [(w, m) for w in range(2) for m in turn]
+    sums = {}
+
+    def add(name, term):
+        sums[name] = sums[name] + term if name in sums else term
+
+    def front(t):
+        x_t = rows_of(0, t)
+        add("gate", dot_nn(x_t, gate_v[cut(t), :]))
+        add("up", dot_nn(x_t, up_v[cut(t), :]))
+
+    def gates():
+        gate_pre, up_pre = sums["gate"], sums["up"]
+        s_lane = iota((1, padded), 1)
+        w_row = jnp.zeros((1, padded), f32)
+        for m in range(peers):
+            row = spare_all[0, m].astype(f32)[2 * spare : 2 * spare + 1, 0:padded]
+            w_row = jnp.where(in_block(s_lane, m), row, w_row)
+        eye_b = (iota((slots, padded), 0) == iota((slots, padded), 1)).astype(f32).astype(bf16)
+        weight_col = dot_nt(eye_b, jnp.broadcast_to(w_row, (group, padded)).astype(bf16))[:, 0:1]
+        gate_clip = jnp.minimum(gate_pre, clamp_limit)
+        up_clip = jnp.clip(up_pre, -clamp_limit, clamp_limit)
+        sigmoid_gate = jax.nn.sigmoid(alpha_gate * gate_clip)
+        swish_gate = gate_clip * sigmoid_gate
+        hidden = (up_clip + 1.0) * swish_gate
+        slope = sigmoid_gate + alpha_gate * swish_gate * (1.0 - sigmoid_gate)
+        weighted_v[...] = (hidden * weight_col).astype(bf16)
+        gate_fac = jnp.where(gate_pre < clamp_limit, weight_col * (up_clip + 1.0) * slope, 0.0)
+        up_fac = jnp.where(jnp.abs(up_pre) < clamp_limit, weight_col * swish_gate, 0.0)
+        return hidden, gate_fac, up_fac
+
+    hooks = [
+        (peers, lambda: front(tp)),
+        (peers + 1, lambda: (settle(core_a, 0), front(core_tp))),
+        (peers + relay_lag, lambda: front(y_tp)),
+        (peers + relay_lag + 1, lambda: (settle(core_b, 0), front(far_tp))),
+        (peers + relay_lag + 2, lambda: factors.append(gates())),
+    ]
+    factors = []
+    for i in range(2 * peers + relay_lag):
+        if i < 2 * peers:
+            forward(*items[i])
+        if i >= relay_lag:
+            relay(*items[i - relay_lag])
+        if i == peers:
+            for load in loads:
+                load.wait()
+        for when, hook in hooks:
+            if when == i:
+                hook()
+    hidden, gate_fac, up_fac = factors[0]
+    back = dot_nt(rows_of(1, tp), down_v[:, cut(tp)])
+    settle(core_a, 1)
+    back = back + dot_nt(rows_of(1, core_tp), down_v[:, cut(core_tp)])
+    back = back + dot_nt(rows_of(1, y_tp), down_v[:, cut(y_tp)])
+    settle(core_b, 1)
+    back = back + dot_nt(rows_of(1, far_tp), down_v[:, cut(far_tp)])
+    gate_grad = (back * gate_fac).astype(bf16)
+    up_grad = (back * up_fac).astype(bf16)
+
+    def piece(t):
+        return dot_nt(gate_grad, gate_v[cut(t), :]) + dot_nt(up_grad, up_v[cut(t), :])
+
+    part[2] = piece(far_tp).astype(bf16)
+    rs_far = remote(part.at[2], core_part.at[0], rs_s.at[0], rs_r.at[0], core_dev)
+    part[3] = piece(core_tp).astype(bf16)
+    rs_near = remote(part.at[3], core_part.at[1], rs_s.at[1], rs_r.at[1], core_dev)
+    mine = piece(y_tp).astype(bf16).astype(f32)
+    rs_far.wait_recv()
+    y_send[...] = (mine + core_part[0].astype(f32)).astype(bf16)
+    ry = []
+    for q, (lo, hi) in enumerate(chunks):
+        rows = pl.ds(lo * main, (hi - lo) * main + (spare_rows if hi == peers else 0))
+        ry.append(remote(y_send.at[rows], y_part.at[rows], ry_s.at[q], ry_r.at[q], y_dev))
+    scores = jnp.sum(hidden * back, axis=1, keepdims=True)
+    eye = iota((slots, padded), 0) == iota((slots, padded), 1)
+    score_own[...] = jnp.sum(jnp.where(eye, scores, 0.0), axis=0, keepdims=True)
+    small = remote(score_own, score_core, sc_s, sc_r, core_dev)
+    mine = piece(tp).astype(bf16).astype(f32)
+    rs_near.wait_recv()
+    part[0] = mine.astype(bf16)
+    small.wait_recv()
+    score_sum[...] = score_own[...] + score_core[...]
+    small_y = remote(score_sum, score_y, sy_s, sy_r, y_dev)
+    returns = []
+    for q, (lo, hi) in enumerate(chunks):
+        row_lo, row_n = lo * main, (hi - lo) * main
+        row_n = row_n + (spare_rows if hi == peers else 0)
+        ry[q].wait_recv()
+        total = (
+            part[0, row_lo : row_lo + row_n, :].astype(f32)
+            + core_part[1, row_lo : row_lo + row_n, :].astype(f32)
+            + y_part[row_lo : row_lo + row_n, :].astype(f32)
+        )
+        ret_send[lo:hi] = total[: (hi - lo) * main].astype(bf16).reshape(hi - lo, main, width)
+        for m in range(max(lo, 1), hi):
+            returns.append(remote(ret_send.at[m], ret_recv.at[m], ret_s.at[m], ret_r.at[m], ep_dev(m)))
+        if hi == peers:
+            for m in range(peers):
+                for x in range(spare):
+                    j = (hi - lo) * main + m * spare + x
+                    ret_spare_send[m, x : x + 1] = total[j : j + 1]
+            for m in range(1, peers):
+                returns.append(
+                    remote(ret_spare_send.at[m], ret_spare_recv.at[m], ret_es.at[m], ret_er.at[m], ep_dev(m))
+                )
+    small_y.wait_recv()
+    score_send[...] = score_sum[...] + score_y[...]
+    for m in range(1, peers):
+        returns.append(remote(score_send, score_recv.at[m], ret_ss.at[m], ret_sr.at[m], ep_dev(m)))
+    weighted = weighted_v[...]
+    for t in range(tp_size):
+        down_out[0, :, t * width : (t + 1) * width] = dot_tn(weighted, rows_of(1, t)).astype(bf16)
+    for copy in returns:
+        copy.wait_recv()
+    back_rows = [ret_send[0]] + [ret_recv[m] for m in range(1, peers)]
+    tile = jnp.zeros((spare_rows, width), f32)
+    s_lane = iota((1, padded), 1)
+    group_row = iota((group, padded), 0)
+    score_mat = jnp.zeros((group, padded), f32)
+    for m in range(peers):
+        block = ret_spare_send[0] if m == 0 else ret_spare_recv[m]
+        for x in range(spare):
+            tile = jnp.where(wide_row == m * spare + x, block[x : x + 1], tile)
+        row = score_send[...] if m == 0 else score_recv[m]
+        score_mat = jnp.where(group_row == m, jnp.where(in_block(s_lane, m), row, 0.0), score_mat)
+    back_all = jnp.concatenate(back_rows + [tile.astype(bf16)], axis=0)
+    token_out[...] = dot_tn(pick, back_all).astype(bf16)
+    found = dot_nn(score_mat.astype(bf16), pick_pad)
+    row0 = jnp.sum(first * found, axis=0, keepdims=True)
+    row1 = jnp.sum(second * found, axis=0, keepdims=True)
+    weight_out[...] = jnp.where(iota((2, tok), 0) == 0, row0, row1).astype(bf16)
+    for copy in pending:
+        copy.wait_send()
+
+
+def fused(tokens, cotangent, routes, route_weights, gate_weight, up_weight, down_weight):
+    peers = lax.axis_size("ep")
+    tp_size = lax.axis_size("tp")
+    tok, top_count = routes.shape
+    width = tokens.shape[1]
+    cap = tok * top_count // peers + 1
+    main = cap // 16 * 16
+    spare = cap - main
+    spare_rows = -(-(peers * spare) // 16) * 16
+    total = peers * main + spare_rows
+    padded = -(-total // 128) * 128
+    hid, full = down_weight.shape[1], down_weight.shape[2]
+    order = send_order if len(send_order) == peers - 1 else tuple(range(1, peers))
+    pieces = min(4, peers)
+    chunks = [(q * peers // pieces, (q + 1) * peers // pieces) for q in range(pieces)]
+    bf16, f32 = jnp.bfloat16, jnp.float32
+    vm = pltpu.VMEM
+    dma = pltpu.SemaphoreType.DMA
+    any_spec = pl.BlockSpec(memory_space=pl.ANY)
+    v_spec = pl.BlockSpec(memory_space=pltpu.VMEM)
+    spare_h = 2 * spare + 1
+    token_grad, weight_grad, down_grad = pl.pallas_call(
+        functools.partial(fused_kernel, peers, main, spare, spare_rows, order, chunks),
+        out_shape=(
+            pltpu.VMEM((tok, width), bf16),
+            pltpu.VMEM((top_count, tok), bf16),
+            pltpu.VMEM((1, hid, full), bf16),
+        ),
+        in_specs=[v_spec] * 4 + [any_spec] * 3,
+        out_specs=(v_spec, v_spec, v_spec),
+        scratch_shapes=[
+            vm((full, hid), bf16), vm((full, hid), bf16), vm((hid, full), bf16),
+            vm((2, peers, main, width), bf16), vm((peers, spare_h, width), bf16),
+            vm((2, tp_size, peers, main, width), bf16), vm((tp_size, peers, spare_h, width), bf16),
+            vm((4, total, width), bf16), vm((2, total, width), bf16),
+            vm((total, width), bf16), vm((total, width), bf16),
+            vm((peers, main, width), bf16), vm((peers, main, width), bf16),
+            vm((peers, spare, width), f32), vm((peers, spare, width), f32),
+            vm((1, padded), f32), vm((1, padded), f32), vm((1, padded), f32),
+            vm((1, padded), f32), vm((1, padded), f32), vm((peers, 1, padded), f32),
+            vm((total, hid), bf16),
+            dma((3,)),
+        ]
+        + [dma((2, peers))] * 2 + [dma((peers,))] * 2
+        + [dma((2, peers))] * 2 + [dma((peers,))] * 2
+        + [dma((2, 2, peers))] * 2 + [dma((2, peers))] * 2
+        + [dma((2,))] * 2 + [dma((len(chunks),))] * 2
+        + [dma] * 4
+        + [dma((peers,))] * 6,
+        compiler_params=pltpu.CompilerParams(collective_id=0, has_side_effects=True),
+    )(tokens, cotangent, routes.T, route_weights.T, gate_weight, up_weight, down_weight)
+    return token_grad, weight_grad.T, down_grad
+
+
+def per_device(tokens, cotangent, routes, route_weights, gate_weight, up_weight, down_weight):
+    args = (tokens, cotangent, routes, route_weights, gate_weight, up_weight, down_weight)
+    cap = routes.shape[0] * routes.shape[1] // lax.axis_size("ep") + 1
+    peers = lax.axis_size("ep")
+    small = cap < 16 or cap % 16 == 0 or cap > 127 or peers & (peers - 1) != 0
+    if small or lax.axis_size("tp") != 4 or routes.shape[1] != 2 or peers > 16:
+        return native(*args)
+    return fused(*args)
+
+
 def solution(mesh):
     placed = (
         P("ep", "tp"),

time: 126 us -> 48.8 us (0.39)
  blocking collectives: 46.7 us -> 0 us
  Pallas kernels: 0 us -> 45.9 us
  waiting for transfers between devices: 22.2 us -> 0 us
  local copies, waits for them, and re-layouts: 18.3 us -> 2.14 us
  between operations: 14 us -> 0.64 us
  starting transfers between devices: 11.3 us -> 0 us
  matrix products: 9.68 us -> 0 us
  other arithmetic: 2.92 us -> 0 us
    pallas_call x0 -> x1, Pallas kernels: none -> 45.9 us  [fused(): pl.pallas_call(functools.partial(fused_kernel, peers, main, spare, spare_...]
    all_to_all x3 -> x0, blocking collectives: 40.9 us -> none  [the longest x1 18 us: per_device(): lax.all_to_all(send_rows, 'ep', split_axis=0, concat_axis=0, tiled=True)]
    reduce_scatter x1 -> x0, waiting for transfers between devices: 12.9 us -> none  [per_device(): lax.psum_scatter(token_part.astype(jnp.bfloat16), 'tp', scatter_dimension...]
    all_to_all x2 -> x0, starting transfers between devices: 11.2 us -> none  [the longest x1 5.66 us: per_device(): lax.all_to_all(score_total.astype(jnp.bfloat16), 'ep', split_axis=0, conc...]
    dot_general x6 -> x0, matrix products: 9.68 us -> none  [the longest x1 3.07 us: expert_terms(): lax.dot_general(weighted, exp_grads, (((0,), (0,)), ((), ())), preferred_...]
    gather x7 -> x0, local copies, waits for them, and re-layouts: 9.63 us -> none  [the longest x1 2.37 us: per_device(): send_scales = jnp.where(filled, route_weights.reshape(-1)[pair_index], 0)]
    psum x1 -> x0, blocking collectives: 5.89 us -> none  [per_device(): score_total = lax.psum(scores, 'tp')]
    all_gather x2 -> x0, waiting for transfers between devices: 4.95 us -> none  [the longest x1 4.95 us: per_device(): lax.all_gather(part_grads, 'tp', axis=1, tiled=True)]
  transfers between devices with their start and end apart: 5 -> 0, of which waited for: 3 -> 0; matrix products, arithmetic and copies ran while one was open for 9% -> 0% of each run, Pallas kernels for 0% -> 0%
where the time goes in v2:
time: 48.8 us; the launch traced here: 48.6 us
  Pallas kernels  45.9 us (94%)
  local copies, waits for them, and re-layouts  2.14 us (4%)
  between operations  0.64 us (1%)
    pallas_call x1, Pallas kernels, fused(): pl.pallas_call(functools.partial(fused_kernel, peers, main, spare, spare_...  45.9 us
    unnamed x3, local copies, waits for them, and re-layouts  2.14 us

profile of v2, /device:TPU:0, one launch (start us, length us, event | category | flops | bytes accessed | tf_op | source)
XLA Modules:
  0.0 48.6 jit_solution(8622706526356791024)
XLA Ops:
  0.6 45.9 %shard_map.94 = (bf16[128,512]{1,0:T(8,128)(2,1)S(1)}, bf16[2,128]{1,0:T(2,128)(2,1)S(1)}, bf16[1,256,2048]{2,1,0:T(8,128)(2,1)S(1)}) custom-call(bf16[128,512]{1,0:T(8,128)(2,1)} %tokens_ref.1, bf16[128,512]{1,0:T(8,128)(2,1)} %cotangent_ref.1, s32[2,128]{1,0:T(2,128)} %bitcast.4, bf16[2,128]{1,0:T(2,128)(2,1)} %bitcast.5, bf16[1,2048,256]{2,1,0:T(8,128)(2,1)} %gate_hbm.1, ...), custom_call_target="tpu_custom_call" | custom-call | tf_op jit(solution)/shard_map/pallas_call | solution.py:460
  46.5 0.7 %copy.13 = bf16[128,512]{1,0:T(8,128)(2,1)} copy(bf16[128,512]{1,0:T(8,128)(2,1)S(1)} %get-tuple-element.9) | data formatting | bytes 262144
  47.2 0.5 %copy.14 = bf16[128,2]{0,1:T(2,128)(2,1)} copy(bf16[128,2]{0,1:T(2,128)(2,1)S(1)} %bitcast.3) | data formatting | bytes 1024
  47.7 1.0 %copy.15 = bf16[1,256,2048]{2,1,0:T(8,128)(2,1)} copy(bf16[1,256,2048]{2,1,0:T(8,128)(2,1)S(1)} %get-tuple-element.11) | data formatting | bytes 2097152

commit v3 on v2

--- a/solution.py
+++ b/solution.py
@@ -10,7 +10,7 @@
 clamp_limit = 7.0
 alpha_gate = 1.702
 send_order = (1, 2, 3, 4, 5, 6, 7)
-relay_lag = 4
+relay_lag = 6
 
 
 def ranks_within(route_block, experts):
@@ -365,25 +365,25 @@
 
     part[2] = piece(far_tp).astype(bf16)
     rs_far = remote(part.at[2], core_part.at[0], rs_s.at[0], rs_r.at[0], core_dev)
+    scores = jnp.sum(hidden * back, axis=1, keepdims=True)
+    eye = iota((slots, padded), 0) == iota((slots, padded), 1)
+    score_own[...] = jnp.sum(jnp.where(eye, scores, 0.0), axis=0, keepdims=True)
+    small = remote(score_own, score_core, sc_s, sc_r, core_dev)
     part[3] = piece(core_tp).astype(bf16)
     rs_near = remote(part.at[3], core_part.at[1], rs_s.at[1], rs_r.at[1], core_dev)
     mine = piece(y_tp).astype(bf16).astype(f32)
+    small.wait_recv()
+    score_sum[...] = score_own[...] + score_core[...]
+    small_y = remote(score_sum, score_y, sy_s, sy_r, y_dev)
     rs_far.wait_recv()
     y_send[...] = (mine + core_part[0].astype(f32)).astype(bf16)
     ry = []
     for q, (lo, hi) in enumerate(chunks):
         rows = pl.ds(lo * main, (hi - lo) * main + (spare_rows if hi == peers else 0))
         ry.append(remote(y_send.at[rows], y_part.at[rows], ry_s.at[q], ry_r.at[q], y_dev))
-    scores = jnp.sum(hidden * back, axis=1, keepdims=True)
-    eye = iota((slots, padded), 0) == iota((slots, padded), 1)
-    score_own[...] = jnp.sum(jnp.where(eye, scores, 0.0), axis=0, keepdims=True)
-    small = remote(score_own, score_core, sc_s, sc_r, core_dev)
     mine = piece(tp).astype(bf16).astype(f32)
     rs_near.wait_recv()
     part[0] = mine.astype(bf16)
-    small.wait_recv()
-    score_sum[...] = score_own[...] + score_core[...]
-    small_y = remote(score_sum, score_y, sy_s, sy_r, y_dev)
     returns = []
     for q, (lo, hi) in enumerate(chunks):
         row_lo, row_n = lo * main, (hi - lo) * main
@@ -395,8 +395,13 @@
             + y_part[row_lo : row_lo + row_n, :].astype(f32)
         )
         ret_send[lo:hi] = total[: (hi - lo) * main].astype(bf16).reshape(hi - lo, main, width)
-        for m in range(max(lo, 1), hi):
+        for m in reversed(range(max(lo, 1), hi)):
             returns.append(remote(ret_send.at[m], ret_recv.at[m], ret_s.at[m], ret_r.at[m], ep_dev(m)))
+        if q == 0:
+            small_y.wait_recv()
+            score_send[...] = score_sum[...] + score_y[...]
+            for m in range(1, peers):
+                returns.append(remote(score_send, score_recv.at[m], ret_ss.at[m], ret_sr.at[m], ep_dev(m)))
         if hi == peers:
             for m in range(peers):
                 for x in range(spare):
@@ -406,10 +411,6 @@
                 returns.append(
                     remote(ret_spare_send.at[m], ret_spare_recv.at[m], ret_es.at[m], ret_er.at[m], ep_dev(m))
                 )
-    small_y.wait_recv()
-    score_send[...] = score_sum[...] + score_y[...]
-    for m in range(1, peers):
-        returns.append(remote(score_send, score_recv.at[m], ret_ss.at[m], ret_sr.at[m], ep_dev(m)))
     weighted = weighted_v[...]
     for t in range(tp_size):
         down_out[0, :, t * width : (t + 1) * width] = dot_tn(weighted, rows_of(1, t)).astype(bf16)
@@ -449,8 +450,8 @@
     padded = -(-total // 128) * 128
     hid, full = down_weight.shape[1], down_weight.shape[2]
     order = send_order if len(send_order) == peers - 1 else tuple(range(1, peers))
-    pieces = min(4, peers)
-    chunks = [(q * peers // pieces, (q + 1) * peers // pieces) for q in range(pieces)]
+    pieces = min(8, peers)
+    chunks = [(q * peers // pieces, (q + 1) * peers // pieces) for q in reversed(range(pieces))]
     bf16, f32 = jnp.bfloat16, jnp.float32
     vm = pltpu.VMEM
     dma = pltpu.SemaphoreType.DMA

time: 48.8 us -> 45.3 us (0.928)
  Pallas kernels: 45.9 us -> 42.3 us
    pallas_call x1, Pallas kernels: 45.9 us -> 42.3 us  [fused(): pl.pallas_call(functools.partial(fused_kernel, peers, main, spare, spare_...]
where the time goes in v3:
time: 45.3 us; the launch traced here: 45.1 us
  Pallas kernels  42.3 us (93%)
  local copies, waits for them, and re-layouts  2.14 us (5%)
  between operations  0.64 us (1%)
    pallas_call x1, Pallas kernels, fused(): pl.pallas_call(functools.partial(fused_kernel, peers, main, spare, spare_...  42.3 us
    unnamed x3, local copies, waits for them, and re-layouts  2.14 us

profile of v3, /device:TPU:0, one launch (start us, length us, event | category | flops | bytes accessed | tf_op | source)
XLA Modules:
  0.0 45.1 jit_solution(16729022155550228116)
XLA Ops:
  0.6 42.3 %shard_map.94 = (bf16[128,512]{1,0:T(8,128)(2,1)S(1)}, bf16[2,128]{1,0:T(2,128)(2,1)S(1)}, bf16[1,256,2048]{2,1,0:T(8,128)(2,1)S(1)}) custom-call(bf16[128,512]{1,0:T(8,128)(2,1)} %tokens_ref.1, bf16[128,512]{1,0:T(8,128)(2,1)} %cotangent_ref.1, s32[2,128]{1,0:T(2,128)} %bitcast.4, bf16[2,128]{1,0:T(2,128)(2,1)} %bitcast.5, bf16[1,2048,256]{2,1,0:T(8,128)(2,1)} %gate_hbm.1, ...), custom_call_target="tpu_custom_call" | custom-call | tf_op jit(solution)/shard_map/pallas_call | solution.py:461
  43.0 0.7 %copy.13 = bf16[128,512]{1,0:T(8,128)(2,1)} copy(bf16[128,512]{1,0:T(8,128)(2,1)S(1)} %get-tuple-element.9) | data formatting | bytes 262144
  43.6 0.5 %copy.14 = bf16[128,2]{0,1:T(2,128)(2,1)} copy(bf16[128,2]{0,1:T(2,128)(2,1)S(1)} %bitcast.3) | data formatting | bytes 1024
  44.2 1.0 %copy.15 = bf16[1,256,2048]{2,1,0:T(8,128)(2,1)} copy(bf16[1,256,2048]{2,1,0:T(8,128)(2,1)S(1)} %get-tuple-element.11) | data formatting | bytes 2097152
